TPU v7x, 128 devices: a whole 4x4x4 slice. The times are simulated.
128 devices in a mesh: sp: 16 (over z, x), tp: 8 (over y, core).
Axes of the slice: x: 4, y: 4, z: 4, core: 2. Of those that a mesh axis runs over, the one named last changes fastest.
Arguments:
- resid: bfloat16 [12288, 2048], P(('sp', 'tp')), may hold values from -6 to 6
- queries: bfloat16 [12288, 1024], P('sp', 'tp'), may hold values from -160 to 160
- keys: bfloat16 [12288, 1024], P('sp', 'tp'), may hold values from -6 to 6
- values: bfloat16 [12288, 1024], P('sp', 'tp'), may hold values from -6 to 6
- cum_gate: float32 [12288, 16], P('sp', 'tp'), may hold values from -1385 to 0, as said below
- out_weight: bfloat16 [1024, 2048], P('tp'), may hold values from -0.375 to 0.375
- norm_gain: float32 [2048], replicated, may hold values from 0.1 to 1.9
- gate_weight: bfloat16 [2048, 5504], P('sp', 'tp'), may hold values from -0.125 to 0.125
- up_weight: bfloat16 [2048, 5504], P('sp', 'tp'), may hold values from -0.125 to 0.125
- down_weight: bfloat16 [5504, 2048], P('tp', 'sp'), may hold values from -0.078125 to 0.078125
Outputs:
- layer_out: bfloat16 [12288, 2048], P(('sp', 'tp'))
Inputs may be any that keep to these rules, and one draw needn't show every extreme that they name: `cum_gate`: each column is non-increasing along positions and starts at or below zero.
All inputs are finite; a program needn't handle non-finite values.
Results may differ from a plain program's by a relative error of at most 0.01.
Values may be sent and summed in bfloat16 or wider, within the bound.
A program may use at most 256 MiB of HBM per device.

v0:
```python
import jax
import jax.numpy as jnp
from jax import lax
from jax.sharding import Mesh
from jax.sharding import PartitionSpec as P

HEAD_DIM = 64
TP = ("tp_0", "tp_1")
SP_TP = ("sp", "tp_0", "tp_1")


def turned_gather(arrays, axis, dims):
    turned = [jnp.moveaxis(a, dim, 0) for a, dim in zip(arrays, dims)]
    widths = [t[0].size for t in turned]
    both = jnp.concatenate([t.reshape(-1, w) for t, w in zip(turned, widths)], axis=1)
    out = lax.all_gather(both, axis, axis=0, tiled=True)
    blocks = jnp.split(out, [sum(widths[:k]) for k in range(1, len(widths))], axis=1)
    return tuple(
        (
            jnp.moveaxis(b.reshape(-1, *t.shape[1:]), 0, dim)
            for b, t, dim in zip(blocks, turned, dims)
        )
    )


def joined_along(blocks, dim):
    blocks = jnp.moveaxis(blocks, 0, dim)
    lengths = blocks.shape
    return blocks.reshape(*lengths[:dim], lengths[dim] * lengths[dim + 1], *lengths[dim + 2 :])


def copy_for_each(value, axis):
    count = lax.axis_size(axis)
    return lax.all_to_all(
        jnp.broadcast_to(value[None], (count, *value.shape)), axis, 0, 0, tiled=True
    )


def gathered_copies(value, axis, dim):
    return joined_along(copy_for_each(value, axis), dim)


def sent_together(arrays, axis, dim, along):
    ends, at = ([], 0)
    for a in arrays[:-1]:
        at += a.shape[along]
        ends.append(at)
    both = jnp.concatenate(arrays, axis=along)
    return tuple(jnp.split(lax.all_gather(both, axis, axis=dim, tiled=True), ends, axis=along))


def sum_by_axis(value, axes, dim):
    for axis in axes:
        value = lax.psum_scatter(value, axis, scatter_dimension=dim, tiled=True)
    return value


def rms_norm(mixed, norm_gain):
    scaled = mixed * lax.rsqrt(jnp.mean(mixed * mixed, axis=-1, keepdims=True) + 1e-06) * norm_gain
    return scaled.astype(jnp.bfloat16)


def rounded(term):
    return term.astype(jnp.bfloat16).astype(jnp.float32)


def local(
    resid,
    queries,
    keys,
    values,
    cum_gate,
    out_weight,
    norm_gain,
    gate_weight,
    up_weight,
    down_weight,
):
    rows = queries.shape[0]
    heads_here = cum_gate.shape[1]
    scale = HEAD_DIM ** (-0.5)
    whole_gate, whole_up, whole_down = turned_gather(
        (gate_weight, up_weight, down_weight), "sp", (0, 0, 1)
    )
    proj_weight = lax.all_gather(out_weight, TP, axis=0, tiled=True)
    first = lax.axis_index("sp") * rows
    gates_all = gathered_copies(cum_gate, "sp", 0)
    query_heads = queries.reshape(rows, heads_here, HEAD_DIM)
    query_pos = first + jnp.arange(rows, dtype=jnp.int32)
    query_gate = cum_gate.T
    best = jnp.full((heads_here, rows), -1e30, jnp.float32)
    key_piece, value_piece = sent_together((keys, values), "sp", 0, 1)
    count = key_piece.shape[0]
    key_heads = key_piece.reshape(count, heads_here, HEAD_DIM)
    value_heads = value_piece.reshape(count, heads_here, HEAD_DIM)
    key_gate = gates_all.T
    score = (
        jnp.einsum("qhd,khd->hqk", query_heads, key_heads, preferred_element_type=jnp.float32)
        * scale
    )
    score = score + query_gate[:, :, None] - key_gate[:, None, :]
    key_pos = jnp.arange(count, dtype=jnp.int32)
    score = jnp.where(key_pos[None, None, :] <= query_pos[None, :, None], score, -jnp.inf)
    new_best = jnp.maximum(best, jnp.max(score, axis=-1))
    weight = jnp.exp(score - new_best[:, :, None])
    total = jnp.sum(weight, axis=-1)
    numer = jnp.einsum(
        "hqk,khd->hqd", weight.astype(jnp.bfloat16), value_heads, preferred_element_type=jnp.float32
    )
    best, total, numer = (new_best, total, numer)
    attn = (
        (numer / total[:, :, None])
        .transpose(1, 0, 2)
        .reshape(rows, heads_here * HEAD_DIM)
        .astype(jnp.bfloat16)
    )
    groups = lax.axis_size(TP)
    share = rows // groups
    own_rows = lax.all_to_all(attn, TP, split_axis=0, concat_axis=1, tiled=True)
    group_width = attn.shape[1]
    row_groups = own_rows.reshape(share, groups, group_width)
    weight_groups = proj_weight.reshape(groups, group_width, proj_weight.shape[1])
    terms = jnp.einsum(
        "rgc,gcd->grd", row_groups, weight_groups, preferred_element_type=jnp.float32
    )
    proj = jnp.sum(rounded(terms), axis=0)
    mixed = resid.astype(jnp.float32) + proj
    normed_all = lax.all_gather(rms_norm(mixed, norm_gain), TP, axis=0, tiled=True)
    gate = jnp.dot(normed_all, whole_gate, preferred_element_type=jnp.float32)
    upper = jnp.dot(normed_all, whole_up, preferred_element_type=jnp.float32)
    hidden = (jax.nn.silu(gate) * upper).astype(jnp.bfloat16)
    ffn_part = jnp.dot(hidden, whole_down, preferred_element_type=jnp.float32)
    ffn = sum_by_axis(rounded(ffn_part).astype(jnp.bfloat16), TP, 0).astype(jnp.float32)
    return (mixed + 0.5 * ffn).astype(jnp.bfloat16)


def solution(mesh):
    split = Mesh(mesh.devices.reshape(mesh.shape["sp"], 4, 2), ("sp", "tp_0", "tp_1"))
    return jax.shard_map(
        local,
        mesh=split,
        in_specs=(
            P(SP_TP, None),
            P("sp", TP),
            P("sp", TP),
            P("sp", TP),
            P("sp", TP),
            P(TP, None),
            P(),
            P("sp", TP),
            P("sp", TP),
            P(TP, "sp"),
        ),
        out_specs=P(SP_TP, None),
        check_vma=False,
    )
```

profile of v0, /device:TPU:1, one launch (start us, length us, event | category | flops | bytes accessed | tf_op | source)
XLA Modules:
  0.0 297.3 jit_solution(10596566933157385455)
XLA Ops:
  6.5 1.8 pad_maximum_fusion.1
  8.4 0.0 all-gather.7.cloned.1.call-start
  8.4 0.7 all-gather.7.cloned.1.call-update
  9.1 1.4 broadcast_in_dim.17
  10.5 8.4 %all-to-all-start = ((f32[16,768,2]{1,2,0:T(2,128)}), f32[16,768,2]{1,2,0:T(2,128)S(1)}, u32[]{:S(2)}, u32[]{:S(2)}) async-start(f32[16,768,2]{1,2,0:T(2,128)} %broadcast_in_dim.17), calls=%async_computation | async-start | bytes 196608 | tf_op jit(solution)/shard_map/all_to_all | solution.py:34
  18.9 0.0 all-gather.11.cloned.1.call-start
  19.0 1.9 pad_maximum_fusion
  20.9 7.4 %iota_compare_fusion = pred[768,12288]{0,1:T(8,128)(4,1)} fusion(s32[768]{0:T(1024)S(1)} %iota_add_fusion), kind=kLoop, calls=%fused_computation.5 | loop fusion | flops 9437184 | bytes 9440256 | tf_op jit(solution)/shard_map/le | solution.py:103
  28.3 0.1 copy.22
  28.4 45.5 %all-gather.5.cloned.1.call-done = bf16[12288,256]{1,0:T(8,128)(2,1)} async-done(((bf16[768,256]{1,0:T(8,128)(2,1)}), bf16[12288,256]{1,0:T(8,128)(2,1)}) %all-gather.5.cloned.1.call-update) | async-done | bytes 6291472 | tf_op jit(solution)/shard_map/all_gather | solution.py:49
  73.9 4.3 %fusion.29 = (bf16[12288,128]{1,0:T(8,128)(2,1)}, bf16[12288,128]{1,0:T(8,128)(2,1)S(1)}) fusion(bf16[12288,256]{1,0:T(8,128)(2,1)} %all-gather.5.cloned.1.call-done), kind=kLoop, calls=%fused_computation.34 | loop fusion | bytes 12582912 | tf_op jit(solution)/shard_map/split | solution.py:49
  78.2 4.7 %copy.21 = bf16[12288,128]{0,1:T(8,128)(2,1)} copy(bf16[12288,128]{1,0:T(8,128)(2,1)} %get-tuple-element.5) | data formatting | bytes 6291456 | tf_op jit(solution)/shard_map/split | solution.py:49
  83.0 33.3 %fusion.2 = (f32[2,768]{1,0:T(2,128)S(1)}, f32[2,12288,768]{2,1,0:T(8,128)}) fusion(f32[2,12288]{1,0:T(2,128)S(1)} %bitcast.45, f32[2,768]{1,0:T(2,128)S(1)} %bitcast.50, pred[768,12288]{0,1:T(8,128)(4,1)} %iota_compare_fusion, bf16[12288,2,64]{0,2,1:T(8,128)(2,1)} %bitcast.43, bf16[768,2,64]{0,2,1:T(8,128)(2,1)S(1)} %bitcast.48), kind=kOutput, calls=%fused_computation.4 | convolution fusion | flops 2510289408 | bytes 88387584 | tf_op jit(solution)/shard_map/qhd,khd->hqk/dot_general | solution.py:98
  116.2 2.8 copy.23
  119.1 27.7 %fusion = f32[2,768]{1,0:T(2,128)S(1)} fusion(f32[2,12288,768]{2,1,0:T(8,128)} %get-tuple-element.8, f32[2,768]{1,0:T(2,128)S(1)} %broadcast_maximum_fusion, f32[2,12288]{1,0:T(2,128)S(1)} %bitcast.46, f32[2,768]{1,0:T(2,128)S(1)} %bitcast.51, pred[768,12288]{0,1:T(8,128)(4,1)} %iota_compare_fusion), kind=kLoop, calls=%fused_computation.2 | loop fusion | flops 113244672 | bytes 85051392 | tf_op jit(solution)/shard_map/reduce_sum | solution.py:106
  146.8 30.7 %fusion.22 = bf16[768,2,64]{0,2,1:T(8,128)(2,1)S(1)} fusion(bf16[12288,2,64]{0,2,1:T(8,128)(2,1)S(1)} %bitcast.44, f32[2,12288,768]{2,1,0:T(8,128)} %get-tuple-element.8, f32[2,768]{1,0:T(2,128)S(1)} %broadcast_maximum_fusion, f32[2,12288]{1,0:T(2,128)S(1)} %bitcast.47, f32[2,768]{1,0:T(2,128)S(1)} %bitcast.52, pred[768,12288]{0,1:T(8,128)(4,1)} %iota_compare_fusion, ...), kind=kOutput, calls=%fused_computation.20 | convolution fusion | flops 2529361920 | bytes 88393728 | tf_op jit(solution)/shard_map/hqk,khd->hqd/dot_general | solution.py:107
  177.5 0.3 convert_element_type.39
  177.8 0.9 copy.25
  178.7 5.0 %all-to-all-start.1 = ((bf16[8,96,128]{2,1,0:T(8,128)(2,1)}), bf16[8,96,128]{2,1,0:T(8,128)(2,1)S(1)}, u32[]{:S(2)}, u32[]{:S(2)}) async-start(bf16[8,96,128]{2,1,0:T(8,128)(2,1)} %copy.25), calls=%async_computation.1 | async-start | bytes 393216 | tf_op jit(solution)/shard_map/all_to_all | solution.py:119
  183.8 5.9 %all-to-all-done.1 = bf16[8,96,128]{2,1,0:T(8,128)(2,1)S(1)} async-done(((bf16[8,96,128]{2,1,0:T(8,128)(2,1)}), bf16[8,96,128]{2,1,0:T(8,128)(2,1)S(1)}, u32[]{:S(2)}, u32[]{:S(2)}) %all-to-all-start.1) | async-done | bytes 196640 | tf_op jit(solution)/shard_map/all_to_all | solution.py:119
  189.6 3.2 %convert_reduce_fusion = f32[96,2048]{1,0:T(8,128)S(1)} fusion(bf16[8,128,2048]{2,1,0:T(8,128)(2,1)} %bitcast.42, bf16[8,96,128]{2,1,0:T(8,128)(2,1)S(1)} %all-to-all-done.1), kind=kOutput, calls=%fused_computation.8 | convolution fusion | flops 407175168 | bytes 5177344 | tf_op jit(solution)/shard_map/rgc,gcd->grd/dot_general | solution.py:123
  192.8 0.2 multiply_reduce_fusion
  193.0 0.9 multiply_convert_fusion.1
  193.9 0.2 reduce-scatter.3.cloned.1.call-start
  194.2 0.0 all-gather.11.cloned.1.call-done
  194.2 26.3 %all-gather.9.cloned.1.call-done = bf16[768,2048]{1,0:T(8,128)(2,1)} async-done(((bf16[96,2048]{1,0:T(8,128)(2,1)}), bf16[768,2048]{1,0:T(8,128)(2,1)}) %all-gather.9.cloned.1.call-update) | async-done | bytes 3145744 | tf_op jit(solution)/shard_map/all_gather | solution.py:128
  220.5 5.1 %fusion.9 = f32[768,688]{0,1:T(8,128)S(1)} fusion(bf16[768,2048]{1,0:T(8,128)(2,1)} %all-gather.9.cloned.1.call-done, bf16[2048,2064]{0,1:T(8,128)(2,1)} %all-gather.11.cloned.1.call-done), kind=kOutput, calls=%fused_computation.14 | convolution fusion | flops 2164260864 | bytes 8077312 | tf_op jit(solution)/shard_map/dot_general | solution.py:129
  225.6 11.7 %convolution_convert_fusion = bf16[768,2048]{1,0:T(8,128)(2,1)} fusion(bf16[2048,2064]{0,1:T(8,128)(2,1)} %all-gather.11.cloned.1.call-done, f32[768,688]{0,1:T(8,128)S(1)} %fusion.9, bf16[768,2048]{1,0:T(8,128)(2,1)} %all-gather.9.cloned.1.call-done), kind=kOutput, calls=%fused_computation.9 | convolution fusion | flops 4333264896 | bytes 14041088 | tf_op jit(solution)/shard_map/dot_general | solution.py:132
  237.3 0.0 reduce-scatter.5.cloned.1.call-start
  237.4 37.9 %reduce-scatter.3.cloned.1.call-done = bf16[192,2048]{1,0:T(8,128)(2,1)} async-done(((bf16[768,2048]{1,0:T(8,128)(2,1)}), bf16[192,2048]{1,0:T(8,128)(2,1)}) %reduce-scatter.3.cloned.1.call-update) | async-done | bytes 786448 | tf_op jit(solution)/shard_map/reduce_scatter | solution.py:54
  275.3 13.3 %reduce-scatter.5.cloned.1.call-done = bf16[96,2048]{1,0:T(8,128)(2,1)} async-done(((bf16[192,2048]{1,0:T(8,128)(2,1)}), bf16[96,2048]{1,0:T(8,128)(2,1)}) %reduce-scatter.5.cloned.1.call-update) | async-done | bytes 393232 | tf_op jit(solution)/shard_map/reduce_scatter | solution.py:54
  288.6 1.9 add_convert_fusion
  (22 shorter events, 0.1 us)
Async XLA Ops:
  6.5 67.4 %all-gather.5.cloned.1.call-start = ((), (), s32[]{:S(2)}) async-start(), calls=%async_computation.4 | async-start | bytes 6684672 | tf_op jit(solution)/shard_map/all_gather | solution.py:49
  8.3 19.9 %copy-start.2 = (bf16[768,128]{1,0:T(8,128)(2,1)S(1)}, bf16[768,128]{1,0:T(8,128)(2,1)}, u32[]{:S(2)}) copy-start(bf16[768,128]{1,0:T(8,128)(2,1)} %param.11) | copy-start | bytes 589828
  8.4 175.4 %all-gather.7.cloned.1.call-start = ((), (), s32[]{:S(2)}) async-start(), calls=%async_computation.5 | async-start | bytes 4718592 | tf_op jit(solution)/shard_map/all_gather | solution.py:85
  10.5 72.5 %all-to-all-start = ((f32[16,768,2]{1,2,0:T(2,128)}), f32[16,768,2]{1,2,0:T(2,128)S(1)}, u32[]{:S(2)}, u32[]{:S(2)}) async-start(f32[16,768,2]{1,2,0:T(2,128)} %broadcast_in_dim.17), calls=%async_computation | async-start | bytes 196608 | tf_op jit(solution)/shard_map/all_to_all | solution.py:34
  18.9 175.3 %all-gather.11.cloned.1.call-start = ((), (), s32[]{:S(2)}) async-start(), calls=%async_computation.7 | async-start | bytes 8982528 | tf_op jit(solution)/shard_map/all_gather | solution.py:16
  78.2 4.7 %copy-start.3 = (f32[768,2]{0,1:T(2,128)S(1)}, f32[768,2]{0,1:T(2,128)}, u32[]{:S(2)}) copy-start(f32[768,2]{0,1:T(2,128)} %param.14) | copy-start | bytes 18436
  119.1 27.8 %copy-start.1 = (bf16[12288,128]{0,1:T(8,128)(2,1)S(1)}, bf16[12288,128]{0,1:T(8,128)(2,1)}, u32[]{:S(2)}) copy-start(bf16[12288,128]{0,1:T(8,128)(2,1)} %copy.23) | copy-start | bytes 9437188
  177.5 15.3 %copy-start = (bf16[96,2048]{1,0:T(8,128)(2,1)S(1)}, bf16[96,2048]{1,0:T(8,128)(2,1)}, u32[]{:S(2)}) copy-start(bf16[96,2048]{1,0:T(8,128)(2,1)} %param.10) | copy-start | bytes 1179652
  177.5 15.5 %copy-start.4 = (f32[2048]{0:T(1024)S(1)}, f32[2048]{0:T(1024)}, u32[]{:S(2)}) copy-start(f32[2048]{0:T(1024)} %param.16) | copy-start | bytes 24580
  178.7 10.9 %all-to-all-start.1 = ((bf16[8,96,128]{2,1,0:T(8,128)(2,1)}), bf16[8,96,128]{2,1,0:T(8,128)(2,1)S(1)}, u32[]{:S(2)}, u32[]{:S(2)}) async-start(bf16[8,96,128]{2,1,0:T(8,128)(2,1)} %copy.25), calls=%async_computation.1 | async-start | bytes 393216 | tf_op jit(solution)/shard_map/all_to_all | solution.py:119
  183.7 36.7 %all-gather.9.cloned.1.call-start = ((), (), s32[]{:S(2)}) async-start(), calls=%async_computation.6 | async-start | bytes 3538944 | tf_op jit(solution)/shard_map/all_gather | solution.py:128
  193.9 81.3 %reduce-scatter.3.cloned.1.call-start = ((), (), s32[]{:S(2)}) async-start(), calls=%async_computation.8 | async-start | bytes 3932160 | tf_op jit(solution)/shard_map/reduce_scatter | solution.py:54
  237.3 51.2 %reduce-scatter.5.cloned.1.call-start = ((), (), s32[]{:S(2)}) async-start(), calls=%async_computation.9 | async-start | bytes 1179648 | tf_op jit(solution)/shard_map/reduce_scatter | solution.py:54
Sparse Core Ops, SparseCore 0:
  9.5 64.4 all-gather.4
  75.7 32.1 all-gather.6
  110.0 75.8 all-gather.10
  194.1 26.3 all-gather.8
  237.5 37.7 reduce-scatter.2
  277.4 11.0 reduce-scatter.4
where the time goes:
time: 298 us; the launch traced here: 297 us
  waiting for transfers between devices  130 us (44%)
  matrix products  83.9 us (28%)
  other arithmetic  41.8 us (14%)
  local copies, waits for them, and re-layouts  14.5 us (5%)
  starting transfers between devices  13.8 us (5%)
  between operations  13.6 us (5%)
    reduce_scatter x2, waiting for transfers between devices, sum_by_axis(): value = lax.psum_scatter(value, axis, scatter_dimension=dim, tiled=True)  51.1 us
    all_gather x1, waiting for transfers between devices, sent_together(): lax.all_gather(both, axis, axis=dim, tiled=True)  45.5 us
    dot_general x1, matrix products, local(): jnp.einsum('qhd,khd->hqk', query_heads, key_heads, preferred_element_type...  33.3 us
    dot_general x1, matrix products, local(): jnp.einsum('hqk,khd->hqd', weight.astype(jnp.bfloat16), value_heads, pref...  30.7 us
    reduce_sum x1, other arithmetic, local(): total = jnp.sum(weight, axis=-1)  27.7 us
    all_gather x1, waiting for transfers between devices, local(): lax.all_gather(rms_norm(mixed, norm_gain), TP, axis=0, tiled=True)  26.3 us
    split x3, local copies, waits for them, and re-layouts, sent_together(): jnp.split(lax.all_gather(both, axis, axis=dim, tiled=True), ends, axis=al...  11.8 us
    dot_general x1, matrix products, local(): ffn_part = jnp.dot(hidden, whole_down, preferred_element_type=jnp.float32)  11.7 us
  transfers between devices with their start and end apart: 8, of which 5 were waited for; matrix products, arithmetic and copies ran while one was open for 40% of the time, Pallas kernels for 0%

commit v1 on v0

v1 whole, which is shorter than its diff:
```python
import functools

import jax
import jax.numpy as jnp
from jax import lax
from jax.experimental import pallas as pl
from jax.experimental.pallas import tpu as pltpu
from jax.sharding import PartitionSpec as P

HEAD_DIM = 64
ROWS = 768
OWN = 96
D = 2048
FFW = 688
GUW = 1408
N_SP = 16
LOOK = 3
BF = jnp.bfloat16
F32 = jnp.float32
MESH = pl.DeviceIdType.MESH
NT = (((1,), (1,)), ((), ()))

N_PIECE = 7
SIGN = (1, 1, -1, 1, -1, 1, -1)


def gray(n):
    return n + (n // 2) * (1 - 2 * (n % 2))


def kernel(
    q_ref, k_ref, v_ref, g_ref, ow_ref, wgu_ref, wd_ref, resid_ref, gain_ref,
    out_ref,
    GG, GK, GV, GW, GD, GO, QZ, ACC, MX, ATL, AT, MIX, NA, HID, SB, RB, PA, TB, RR,
    rs, ss, ors, oss, nrs, nss, ars, ass, brs, bss, crs, css, lsem,
):
    sp = lax.axis_index("sp")
    tp = lax.axis_index("tp")
    c = tp % 2
    y = tp // 2
    z = sp // 4
    x = sp % 4
    a = z + c * (x - z)
    b = x + c * (z - x)

    def spof(da, db):
        return ((a + da + 4) % 4) * (4 - 3 * c) + ((b + db + 4) % 4) * (1 + 3 * c)

    def tpof(yy, cc):
        return yy * 2 + cc

    sib = tpof(y, 1 - c)

    bar = pltpu.get_barrier_semaphore()
    for da, db in ((1, 0), (3, 0), (0, 1), (0, 3)):
        pl.semaphore_signal(bar, inc=1, device_id=(spof(da, db), tp), device_id_type=MESH)
    for i in range(1, 8):
        pl.semaphore_signal(bar, inc=1, device_id=(sp, (tp + i) % 8), device_id_type=MESH)

    def part(p, s):
        if p == 0:
            return GG.at[s]
        if p == 1:
            return GK.at[pl.ds(pl.multiple_of(s * ROWS, ROWS), ROWS)]
        if p == 2:
            return GV.at[pl.ds(pl.multiple_of(s * ROWS, ROWS), ROWS)]
        if p == 3:
            return GW.at[pl.ds(pl.multiple_of(s * 128, 64), 64)]
        if p == 4:
            return GW.at[pl.ds(pl.multiple_of(s * 128 + 64, 64), 64)]
        if p == 5:
            return GD.at[pl.ds(0, 352), pl.ds(pl.multiple_of(s * 128, 128), 128)]
        return GD.at[pl.ds(352, 336), pl.ds(pl.multiple_of(s * 128, 128), 128)]

    local = [
        pltpu.make_async_copy(g_ref, part(0, sp), lsem.at[0]),
        pltpu.make_async_copy(k_ref, part(1, sp), lsem.at[1]),
        pltpu.make_async_copy(v_ref, part(2, sp), lsem.at[2]),
        pltpu.make_async_copy(wgu_ref, GW.at[pl.ds(pl.multiple_of(sp * 128, 128), 128)], lsem.at[3]),
        pltpu.make_async_copy(wd_ref, GD.at[:, pl.ds(pl.multiple_of(sp * 128, 128), 128)], lsem.at[4]),
        pltpu.make_async_copy(ow_ref, GO.at[pl.ds(pl.multiple_of(tp * 128, 128), 128)], lsem.at[5]),
    ]
    for cp in local:
        cp.start()

    def copy(p, s, idx, dst):
        return pltpu.make_async_remote_copy(
            src_ref=part(p, s), dst_ref=part(p, s), send_sem=ss.at[p, idx], recv_sem=rs.at[p, s],
            device_id=(dst, tp), device_id_type=MESH,
        )

    def begin(p):
        copy(p, sp, 2, spof(0, 1)).start()
        copy(p, sp, 3, spof(0, 3)).start()
        copy(p, sp, 0, spof(1, 0)).start()
        copy(p, sp, 1, spof(3, 0)).start()

    def serve(p, k):
        da = gray(k % 4)
        db = gray(k // 4)
        s = spof(da, db)
        copy(p, s, 0, sp).wait_recv()
        d = SIGN[p]
        back = (4 - d) % 4

        @pl.when((k < 4) & (da == back))
        def _():
            copy(p, s, 10, spof(d, 0)).start()

        @pl.when(k < 4)
        def _():
            copy(p, s, 2 + 2 * k, spof(0, 1)).start()
            copy(p, s, 3 + 2 * k, spof(0, 3)).start()

        @pl.when(db == back)
        def _():
            copy(p, s, 11 + k % 4, spof(0, d)).start()

    def serve_own(p):
        pass

    dy = 1 - 2 * c

    def yat(n):
        return (y + n + 4) % 4

    def ycopy(block, sems, rsems, idx, slot, dst):
        return pltpu.make_async_remote_copy(
            src_ref=block(slot), dst_ref=block(slot), send_sem=sems.at[idx], recv_sem=rsems.at[slot],
            device_id=(sp, dst), device_id_type=MESH,
        )

    def slot_of(yy, cc):
        return cc * 4 + yy

    def ybegin(block, sems, rsems):
        own = slot_of(y, c)
        ycopy(block, sems, rsems, 0, own, tpof(yat(dy), c)).start()
        ycopy(block, sems, rsems, 1, own, tpof(yat(-dy), c)).start()
        ycopy(block, sems, rsems, 2, own, sib).start()

    def yserve(block, sems, rsems, n):
        if n == 0:
            s = slot_of(yat(-dy), c)
            ycopy(block, sems, rsems, 0, s, sib).wait_recv()
            ycopy(block, sems, rsems, 3, s, tpof(yat(dy), c)).start()
            ycopy(block, sems, rsems, 4, s, sib).start()
        elif n == 1:
            s = slot_of(yat(dy), c)
            ycopy(block, sems, rsems, 0, s, sib).wait_recv()
            ycopy(block, sems, rsems, 5, s, sib).start()
        else:
            s = slot_of(yat(2), c)
            ycopy(block, sems, rsems, 0, s, sib).wait_recv()
            ycopy(block, sems, rsems, 6, s, sib).start()

    def yfinish(block, sems, rsems):
        for n in range(4):
            s = slot_of(yat(n), 1 - c)
            ycopy(block, sems, rsems, 0, s, sib).wait_recv()

    def oblock(slot):
        t = (slot % 4) * 2 + slot // 4
        return GO.at[pl.ds(pl.multiple_of(t * 128, 128), 128)]

    def nblock(slot):
        return NA.at[pl.ds(pl.multiple_of(slot * OWN, OWN), OWN)]

    lane = lax.broadcasted_iota(jnp.int32, (ROWS, 128), 1)
    qs = q_ref[...].astype(F32) * (HEAD_DIM ** (-0.5))
    QZ[0] = jnp.where(lane < HEAD_DIM, qs, 0.0).astype(BF)
    QZ[1] = jnp.where(lane >= HEAD_DIM, qs, 0.0).astype(BF)

    for cp in local:
        cp.wait()
    pl.semaphore_wait(bar, 11)
    for p in (1, 2, 0):
        begin(p)
    ybegin(oblock, oss, ors)

    def scores(h, r0, n, s, width):
        qh = QZ[h, pl.ds(r0, n), :]
        kb = GK[pl.ds(pl.multiple_of(s * ROWS, ROWS), width), :]
        sc = lax.dot_general(qh, kb, NT, preferred_element_type=F32)
        return sc - GG[s, h : h + 1, :width]

    def values_of(s, width):
        vb = GV[pl.ds(pl.multiple_of(s * ROWS, ROWS), width), :]
        return jnp.concatenate([vb, jnp.ones((width, 128), BF)], axis=1)

    QB = 256
    for i in range(ROWS // QB):
        width = QB * (i + 1)
        row = lax.broadcasted_iota(jnp.int32, (QB, width), 0) + i * QB
        col = lax.broadcasted_iota(jnp.int32, (QB, width), 1)
        for h in range(2):
            sc = jnp.where(col <= row, scores(h, i * QB, QB, sp, width), -1e30)
            top = jnp.broadcast_to(jnp.max(sc, axis=1, keepdims=True), (QB, 128))
            wt = jnp.exp(sc - jnp.concatenate([top] * (width // 128), axis=1))
            ACC[h, i * QB : (i + 1) * QB, :] = jnp.dot(
                wt.astype(BF), values_of(sp, width), preferred_element_type=F32
            )
            MX[h, i * QB : (i + 1) * QB, :] = top

    def tile(s):
        def chunk(i, _):
            r0 = pl.multiple_of(i * QB, QB)
            for h in range(2):
                sc = scores(h, r0, QB, s, ROWS)
                old = MX[h, pl.ds(r0, QB), :]
                top = jnp.maximum(old, jnp.max(sc, axis=1, keepdims=True))
                wt = jnp.exp(sc - jnp.concatenate([top] * (ROWS // 128), axis=1))
                fade = jnp.exp(old - top)
                pv = jnp.dot(wt.astype(BF), values_of(s, ROWS), preferred_element_type=F32)
                ACC[h, pl.ds(r0, QB), :] = (
                    ACC[h, pl.ds(r0, QB), :] * jnp.concatenate([fade, fade], axis=1) + pv
                )
                MX[h, pl.ds(r0, QB), :] = top
            return 0

        lax.fori_loop(0, ROWS // QB, chunk, 0)

    KV = (1, 2, 0)
    for k in range(1, LOOK + 1):
        for p in KV:
            serve(p, k)

    def step(k, _):
        @pl.when(k + LOOK < N_SP)
        def _():
            for p in KV:
                serve(p, k + LOOK)

        @pl.when(k == 3)
        def _():
            yserve(oblock, oss, ors, 0)
            yserve(oblock, oss, ors, 1)

        @pl.when(k == 8)
        def _():
            yserve(oblock, oss, ors, 2)
            begin(3)
            begin(4)

        @pl.when(k == 12)
        def _():
            for p in (3, 4):
                for kk in range(1, 4):
                    serve(p, kk)
            begin(5)
            begin(6)

        s = spof(gray(k % 4), gray(k // 4))

        @pl.when(s < sp)
        def _():
            tile(s)

        return 0

    lax.fori_loop(1, N_SP, step, 0)

    first = lax.broadcasted_iota(jnp.int32, (ROWS, 128), 1) < HEAD_DIM
    o0 = ACC[0, :, :128] / ACC[0, :, 128:]
    o1 = ACC[1, :, :128] / ACC[1, :, 128:]
    ATL[...] = jnp.where(first, o0, o1).astype(BF)

    def acopy(i, src, dst, slot):
        return pltpu.make_async_remote_copy(
            src_ref=ATL.at[pl.ds(pl.multiple_of(dst * OWN, 32), OWN)],
            dst_ref=AT.at[:, pl.ds(pl.multiple_of(slot * 128, 128), 128)],
            send_sem=ass.at[i], recv_sem=ars.at[slot], device_id=(sp, dst), device_id_type=MESH,
        )

    for i in range(1, 8):
        acopy(i - 1, tp, (tp + i) % 8, tp).start()
    AT[:, pl.ds(pl.multiple_of(tp * 128, 128), 128)] = ATL[pl.ds(pl.multiple_of(tp * OWN, 32), OWN), :]
    yfinish(oblock, oss, ors)
    for p in (3, 4):
        for kk in range(4, 8):
            serve(p, kk)
    for i in range(1, 8):
        t = (tp + i) % 8
        acopy(0, tp, t, t).wait_recv()

    NB = 512
    sq = jnp.zeros((OWN, 1), F32)
    for j in range(D // NB):
        pj = jnp.dot(AT[...], GO[:, j * NB : (j + 1) * NB], preferred_element_type=F32)
        mj = resid_ref[:, j * NB : (j + 1) * NB].astype(F32) + pj
        MIX[:, j * NB : (j + 1) * NB] = mj
        sq = sq + jnp.sum(mj * mj, axis=1, keepdims=True)
    inv = lax.rsqrt(sq * (1.0 / D) + 1e-6)
    own_slot = slot_of(y, c)
    NA[pl.ds(pl.multiple_of(own_slot * OWN, OWN), OWN), :] = (MIX[...] * inv * gain_ref[...]).astype(BF)
    ybegin(nblock, nss, nrs)
    for p in (5, 6):
        for kk in range(1, 4):
            serve(p, kk)
    for p in (3, 4):
        for kk in range(8, 12):
            serve(p, kk)
    yserve(nblock, nss, nrs, 0)
    yserve(nblock, nss, nrs, 1)
    yserve(nblock, nss, nrs, 2)
    for p in (5, 6):
        for kk in range(4, 12):
            serve(p, kk)
    yfinish(nblock, nss, nrs)
    for p in (3, 4):
        for kk in range(12, 16):
            serve(p, kk)

    def gu(j, _):
        col = pl.multiple_of(j * 256, 256)
        r = jnp.dot(NA[...], GW[:, pl.ds(col, 256)], preferred_element_type=F32)
        gt = r[:, :128]
        HID[:, pl.ds(pl.multiple_of(j * 128, 128), 128)] = (gt / (1.0 + jnp.exp(-gt)) * r[:, 128:]).astype(BF)
        return 0

    lax.fori_loop(0, 5, gu, 0)
    r = jnp.dot(NA[...], GW[:, 1280:1408], preferred_element_type=F32)
    gt = r[:, :48]
    HID[:, 640:688] = (gt / (1.0 + jnp.exp(-gt)) * r[:, 48:96]).astype(BF)
    for p in (5, 6):
        for kk in range(12, 16):
            serve(p, kk)

    half = 4 * OWN

    def scopy(n):
        blk = yat(2 + n)
        view = pl.ds(pl.multiple_of(blk * OWN, OWN), OWN)
        return pltpu.make_async_remote_copy(
            src_ref=SB.at[view], dst_ref=RB.at[view], send_sem=bss.at[blk], recv_sem=brs.at[blk],
            device_id=(sp, sib), device_id_type=MESH,
        )

    hs = HID[pl.ds(pl.multiple_of((1 - c) * half, half), half), :]
    for j in range(D // NB):
        SB[:, j * NB : (j + 1) * NB] = jnp.dot(
            hs, GD[:, j * NB : (j + 1) * NB], preferred_element_type=F32
        ).astype(BF)
    for n in range(4):
        scopy(n).start()
    ho = HID[pl.ds(pl.multiple_of(c * half, half), half), :]
    for j in range(D // NB):
        PA[:, j * NB : (j + 1) * NB] = jnp.dot(ho, GD[:, j * NB : (j + 1) * NB], preferred_element_type=F32)
    for n in range(4):
        scopy(n).wait_recv()

    def both(n):
        view = pl.ds(pl.multiple_of(yat(n) * OWN, OWN), OWN)
        return PA[view, :] + RB[view, :].astype(F32)

    def rcopy(n, to):
        return pltpu.make_async_remote_copy(
            src_ref=TB.at[n], dst_ref=RR.at[n], send_sem=css.at[n], recv_sem=crs.at[n],
            device_id=(sp, tpof(yat(to), c)), device_id_type=MESH,
        )

    TB[0] = both(2).astype(BF)
    rcopy(0, dy).start()
    TB[1] = both(-dy).astype(BF)
    rcopy(1, -dy).start()
    rcopy(0, dy).wait_recv()
    TB[2] = (both(dy) + RR[0].astype(F32)).astype(BF)
    rcopy(2, dy).start()
    rcopy(1, -dy).wait_recv()
    rcopy(2, dy).wait_recv()
    ffn = both(0) + RR[1].astype(F32) + RR[2].astype(F32)
    out_ref[...] = (MIX[...] + 0.5 * ffn).astype(BF)

    for n in range(3):
        rcopy(n, dy).wait_send()
    for n in range(4):
        scopy(n).wait_send()
    for i in range(1, 8):
        acopy(i - 1, tp, (tp + i) % 8, tp).wait_send()
    for i in range(7):
        ycopy(oblock, oss, ors, i, slot_of(y, c), sib).wait_send()
        ycopy(nblock, nss, nrs, i, slot_of(y, c), sib).wait_send()
    for p in range(N_PIECE):

        def drain(i, _):
            copy(p, sp, i, sp).wait_send()
            return 0

        lax.fori_loop(0, 15, drain, 0)


def local(resid, queries, keys, values, cum_gate, out_weight, norm_gain, gate_weight, up_weight, down_weight):
    gates = jnp.pad(cum_gate.T, ((0, 6), (0, 0)))
    cols = []
    for j in range(5):
        cols += [gate_weight[:, j * 128 : (j + 1) * 128], up_weight[:, j * 128 : (j + 1) * 128]]
    cols += [gate_weight[:, 640:], up_weight[:, 640:], jnp.zeros((128, 32), BF)]
    gate_up = jnp.concatenate(cols, axis=1)
    vm = pl.BlockSpec(memory_space=pltpu.VMEM)
    hbm = pl.BlockSpec(memory_space=pl.ANY)
    dma = pltpu.SemaphoreType.DMA
    V = pltpu.VMEM
    return pl.pallas_call(
        kernel,
        out_shape=jax.ShapeDtypeStruct((OWN, D), BF),
        in_specs=[vm, hbm, hbm, hbm, hbm, hbm, hbm, vm, vm],
        out_specs=vm,
        scratch_shapes=[
            V((N_SP, 8, ROWS), F32),
            V((N_SP * ROWS, 128), BF),
            V((N_SP * ROWS, 128), BF),
            V((D, GUW), BF),
            V((FFW, D), BF),
            V((1024, D), BF),
            V((2, ROWS, 128), BF),
            V((2, ROWS, 256), F32),
            V((2, ROWS, 128), F32),
            V((ROWS, 128), BF),
            V((OWN, 1024), BF),
            V((OWN, D), F32),
            V((ROWS, D), BF),
            V((ROWS, FFW), BF),
            V((4 * OWN, D), BF),
            V((4 * OWN, D), BF),
            V((4 * OWN, D), F32),
            V((3, OWN, D), BF),
            V((3, OWN, D), BF),
            dma((N_PIECE, N_SP)),
            dma((N_PIECE, 15)),
            dma((8,)),
            dma((7,)),
            dma((8,)),
            dma((7,)),
            dma((8,)),
            dma((7,)),
            dma((4,)),
            dma((4,)),
            dma((3,)),
            dma((3,)),
            dma((6,)),
        ],
        compiler_params=pltpu.CompilerParams(
            collective_id=0, has_side_effects=True, vmem_limit_bytes=64 * 1024 * 1024 - 128 * 1024
        ),
        name="layer",
    )(queries, keys, values, gates, out_weight, gate_up, down_weight, resid, norm_gain.reshape(1, D))


def solution(mesh):
    return jax.shard_map(
        local,
        mesh=mesh,
        in_specs=(
            P(("sp", "tp"), None),
            P("sp", "tp"),
            P("sp", "tp"),
            P("sp", "tp"),
            P("sp", "tp"),
            P("tp", None),
            P(),
            P("sp", "tp"),
            P("sp", "tp"),
            P("tp", "sp"),
        ),
        out_specs=P(("sp", "tp"), None),
        check_vma=False,
    )
```

time: 298 us -> 150 us (0.50)
  Pallas kernels: 0 us -> 142 us
  waiting for transfers between devices: 130 us -> 0 us
  matrix products: 83.9 us -> 0 us
  other arithmetic: 41.8 us -> 0 us
  starting transfers between devices: 13.8 us -> 0 us
  between operations: 13.6 us -> 0.11 us
  local copies, waits for them, and re-layouts: 14.5 us -> 6.96 us
    pallas_call x0 -> x1, Pallas kernels: none -> 142 us  [local(): pl.pallas_call(kernel, out_shape=jax.ShapeDtypeStruct((OWN, D), BF), in_s...]
    dot_general x5 -> x0, matrix products: 83.9 us -> none  [the longest x1 33.3 us: local(): jnp.einsum('qhd,khd->hqk', query_heads, key_heads, preferred_element_type...]
    all_gather x4 -> x0, waiting for transfers between devices: 71.8 us -> none  [the longest x1 45.5 us: sent_together(): lax.all_gather(both, axis, axis=dim, tiled=True)]
    reduce_scatter x2 -> x0, waiting for transfers between devices: 51.1 us -> none  [sum_by_axis(): value = lax.psum_scatter(value, axis, scatter_dimension=dim, tiled=True)]
    reduce_sum x2 -> x0, other arithmetic: 27.9 us -> none  [the longest x1 27.7 us: local(): total = jnp.sum(weight, axis=-1)]
    all_to_all x2 -> x0, starting transfers between devices: 13.5 us -> none  [the longest x1 8.42 us: copy_for_each(): lax.all_to_all(jnp.broadcast_to(value[None], (count, *value.shape)), axis...]
    split x3 -> x0, local copies, waits for them, and re-layouts: 11.8 us -> none  [sent_together(): jnp.split(lax.all_gather(both, axis, axis=dim, tiled=True), ends, axis=al...]
    le x1 -> x0, other arithmetic: 7.39 us -> none  [local(): key_pos[None, None, :] <= query_pos[None, :, None]]
  transfers between devices with their start and end apart: 8 -> 0, of which waited for: 5 -> 0; matrix products, arithmetic and copies ran while one was open for 40% -> 0% of each run, Pallas kernels for 0% -> 0%
where the time goes in v1:
time: 150 us; the launch traced here: 149 us
  Pallas kernels  142 us (95%)
  local copies, waits for them, and re-layouts  6.96 us (5%)
    pallas_call x1, Pallas kernels, local(): pl.pallas_call(kernel, out_shape=jax.ShapeDtypeStruct((OWN, D), BF), in_s...  142 us
    unnamed x17, local copies, waits for them, and re-layouts  3.2 us

profile of v1, /device:TPU:1, one launch (start us, length us, event | category | flops | bytes accessed | tf_op | source)
XLA Modules:
  0.0 149.3 jit_solution(9190643220460717495)
XLA Ops:
  0.0 0.0 copy-start
  0.0 0.9 fusion.1
  0.9 0.1 copy.23
  1.0 0.0 copy-done
  1.0 0.1 copy.24
  1.1 0.1 copy.25
  1.3 0.1 copy.26
  1.4 0.1 copy.27
  1.5 0.1 copy.28
  1.6 0.1 copy.29
  1.8 0.1 copy.30
  1.9 0.1 copy.31
  2.0 0.1 copy.32
  2.1 0.0 slice-start
  2.2 0.7 slice-done
  2.9 0.1 copy.33
  3.0 0.0 slice-start.1
  3.0 0.7 slice-done.1
  3.7 0.1 copy.34
  3.8 0.0 copy-start.1
  3.8 0.8 concatenate.3.wgu_ref
  4.7 0.0 copy-done.1
  4.7 0.6 pad.4.g_ref
  5.3 142.2 %layer.1 = bf16[96,2048]{1,0:T(8,128)(2,1)} custom-call(bf16[768,128]{1,0:T(8,128)(2,1)} %q_ref.1, bf16[768,128]{1,0:T(8,128)(2,1)} %k_ref.1, bf16[768,128]{1,0:T(8,128)(2,1)} %v_ref.1, f32[8,768]{1,0:T(8,128)} %pad.4.g_ref, bf16[128,2048]{1,0:T(8,128)(2,1)} %ow_ref.1, bf16[128,1408]{1,0:T(8,128)(2,1)} %concatenate.3.wgu_ref, bf16[688,128]{1,0:T(8,128)(2,1)} %wd_ref.1, ...), custom_call_target="tpu_custom_call" | custom-call | tf_op jit(solution)/shard_map/layer/pallas_call | solution.py:403
  147.5 1.8 %copy.36 = bf16[96,2048]{1,0:T(8,128)(2,1)} copy(bf16[96,2048]{1,0:T(8,128)(2,1)} %layer.1) | data formatting | bytes 786432
  (2 shorter events, 0.0 us)
Async XLA Ops:
  0.0 1.0 copy-start
  2.1 0.7 slice-start
  3.0 0.7 slice-start.1
  3.8 0.9 copy-start.1

commit v2 on v1

v2 whole, which is shorter than its diff:
```python
import functools

import jax
import jax.numpy as jnp
from jax import lax
from jax.experimental import pallas as pl
from jax.experimental.pallas import tpu as pltpu
from jax.sharding import PartitionSpec as P

HEAD_DIM = 64
ROWS = 768
OWN = 96
D = 2048
FFW = 688
GUW = 1408
N_SP = 16
HQ = ROWS // 2
KV = (1, 2, 0)
LOOK = 1
K_O1 = 6
K_O2 = 10
K_W = 5
K_WS = 12
WEIGHTS = (3, 4, 5, 6)
BF = jnp.bfloat16
F32 = jnp.float32
MESH = pl.DeviceIdType.MESH
NT = (((1,), (1,)), ((), ()))

N_PIECE = 7
SIGN = (1, 1, -1, 1, -1, 1, -1)


WAVE = (
    (0, 0), (1, 0), (3, 0), (0, 1), (0, 3), (2, 0), (1, 1), (3, 1),
    (1, 3), (3, 3), (0, 2), (2, 1), (2, 3), (1, 2), (3, 2), (2, 2),
)


def offsets(k):
    if isinstance(k, int):
        return WAVE[k]
    da, db = jnp.int32(0), jnp.int32(0)
    for n in range(1, 16):
        da = jnp.where(k == n, WAVE[n][0], da)
        db = jnp.where(k == n, WAVE[n][1], db)
    return da, db


def kernel(
    q_ref, k_ref, v_ref, g_ref, ow_ref, wg_in, wu_in, wd_ref, resid_in, gain_in,
    out_hbm,
    GG, GK, GV, GW, GD, GO, QR, QZ, ACC, MX, ATL, AT, MIX, NA, HID, SB, RB, PA, TB, RR,
    wg_ref, wu_ref, resid_ref, gain_ref, out_ref,
    rs, ss, ors, oss, nrs, nss, ars, ass, brs, bss, crs, css, lsem, qsem, osem,
):
    sp = lax.axis_index("sp")
    tp = lax.axis_index("tp")
    c = tp % 2
    y = tp // 2
    z = sp // 4
    x = sp % 4
    a = z + c * (x - z)
    b = x + c * (z - x)

    def spof(da, db):
        return ((a + da + 4) % 4) * (4 - 3 * c) + ((b + db + 4) % 4) * (1 + 3 * c)

    def tpof(yy, cc):
        return yy * 2 + cc

    sib = tpof(y, 1 - c)
    ps = N_SP - 1 - sp

    bar = pltpu.get_barrier_semaphore()
    for da, db in ((1, 0), (3, 0), (0, 1), (0, 3)):
        pl.semaphore_signal(bar, inc=1, device_id=(spof(da, db), tp), device_id_type=MESH)
    for i in range(8):
        if i:
            pl.semaphore_signal(bar, inc=1, device_id=(sp, (tp + i) % 8), device_id_type=MESH)
        pl.semaphore_signal(bar, inc=1, device_id=(ps, (tp + i) % 8), device_id_type=MESH)

    def part(p, s):
        if p == 0:
            return GG.at[s]
        if p == 1:
            return GK.at[pl.ds(pl.multiple_of(s * ROWS, ROWS), ROWS)]
        if p == 2:
            return GV.at[pl.ds(pl.multiple_of(s * ROWS, ROWS), ROWS)]
        if p == 3:
            return GW.at[pl.ds(pl.multiple_of(s * 128, 64), 64)]
        if p == 4:
            return GW.at[pl.ds(pl.multiple_of(s * 128 + 64, 64), 64)]
        if p == 5:
            return GD.at[pl.ds(0, 352), pl.ds(pl.multiple_of(s * 128, 128), 128)]
        return GD.at[pl.ds(352, 336), pl.ds(pl.multiple_of(s * 128, 128), 128)]

    local = [
        pltpu.make_async_copy(g_ref, part(0, sp), lsem.at[0]),
        pltpu.make_async_copy(k_ref, part(1, sp), lsem.at[1]),
        pltpu.make_async_copy(v_ref, part(2, sp), lsem.at[2]),
        pltpu.make_async_copy(wd_ref, GD.at[:, pl.ds(pl.multiple_of(sp * 128, 128), 128)], lsem.at[3]),
        pltpu.make_async_copy(ow_ref, GO.at[pl.ds(pl.multiple_of(tp * 128, 128), 128)], lsem.at[4]),
        pltpu.make_async_copy(wg_in, wg_ref, lsem.at[5]),
        pltpu.make_async_copy(wu_in, wu_ref, lsem.at[6]),
        pltpu.make_async_copy(resid_in, resid_ref, lsem.at[7]),
        pltpu.make_async_copy(gain_in, gain_ref, lsem.at[8]),
    ]
    for cp in local:
        cp.start()

    def copy(p, s, idx, dst):
        return pltpu.make_async_remote_copy(
            src_ref=part(p, s), dst_ref=part(p, s), send_sem=ss.at[p, idx], recv_sem=rs.at[p, s],
            device_id=(dst, tp), device_id_type=MESH,
        )

    def begin_first(p):
        copy(p, sp, 0, spof(1, 0)).start()
        copy(p, sp, 1, spof(3, 0)).start()

    def send_second(p, da):
        s = spof(da, 0)
        copy(p, s, 2 + 2 * da, spof(0, 1)).start()
        copy(p, s, 3 + 2 * da, spof(0, 3)).start()

    def begin(p):
        begin_first(p)
        send_second(p, 0)

    def serve_first(p, da):
        s = spof(da, 0)
        copy(p, s, 0, sp).wait_recv()
        d = SIGN[p]
        if da == (4 - d) % 4:
            copy(p, s, 10, spof(d, 0)).start()

    def relay(p):
        d = SIGN[p]
        for da in (0, 1, 3, 2):
            s = spof(da, 4 - d)
            copy(p, s, 0, sp).wait_recv()
            copy(p, s, 11 + da, spof(0, d)).start()

    def collect(p):
        d = SIGN[p]
        for db in (4 + d, 2):
            for da in (0, 1, 3, 2):
                copy(p, spof(da, db), 0, sp).wait_recv()

    def serve(p, k):
        da, db = offsets(k)
        s = spof(da, db)
        copy(p, s, 0, sp).wait_recv()
        d = SIGN[p]
        back = (4 - d) % 4

        @pl.when((db == 0) & (da == back))
        def _():
            copy(p, s, 10, spof(d, 0)).start()

        @pl.when(db == 0)
        def _():
            copy(p, s, 2 + 2 * da, spof(0, 1)).start()
            copy(p, s, 3 + 2 * da, spof(0, 3)).start()

        @pl.when(db == back)
        def _():
            copy(p, s, 11 + da, spof(0, d)).start()

    dy = 1 - 2 * c

    def yat(n):
        return (y + n + 4) % 4

    def ycopy(block, sems, rsems, idx, slot, dst):
        return pltpu.make_async_remote_copy(
            src_ref=block(slot), dst_ref=block(slot), send_sem=sems.at[idx], recv_sem=rsems.at[slot],
            device_id=(sp, dst), device_id_type=MESH,
        )

    def slot_of(yy, cc):
        return cc * 4 + yy

    def ybegin(block, sems, rsems):
        own = slot_of(y, c)
        ycopy(block, sems, rsems, 0, own, tpof(yat(dy), c)).start()
        ycopy(block, sems, rsems, 1, own, tpof(yat(-dy), c)).start()
        ycopy(block, sems, rsems, 2, own, sib).start()

    def yserve(block, sems, rsems, n):
        if n == 0:
            s = slot_of(yat(-dy), c)
            ycopy(block, sems, rsems, 0, s, sib).wait_recv()
            ycopy(block, sems, rsems, 3, s, tpof(yat(dy), c)).start()
            ycopy(block, sems, rsems, 4, s, sib).start()
        elif n == 1:
            s = slot_of(yat(dy), c)
            ycopy(block, sems, rsems, 0, s, sib).wait_recv()
            ycopy(block, sems, rsems, 5, s, sib).start()
        else:
            s = slot_of(yat(2), c)
            ycopy(block, sems, rsems, 0, s, sib).wait_recv()
            ycopy(block, sems, rsems, 6, s, sib).start()

    def yfinish(block, sems, rsems):
        for n in range(4):
            s = slot_of(yat(n), 1 - c)
            ycopy(block, sems, rsems, 0, s, sib).wait_recv()

    def oblock(slot):
        t = (slot % 4) * 2 + slot // 4
        return GO.at[pl.ds(pl.multiple_of(t * 128, 128), 128)]

    def nblock(part):
        def view(slot):
            return NA.at[pl.ds(pl.multiple_of(slot * OWN, OWN), OWN), pl.ds(part * (D // 2), D // 2)]

        return view, nss.at[part], nrs.at[part]

    half_lane = lax.broadcasted_iota(jnp.int32, (HQ, 128), 1)

    def spread(half, q):
        qs = q.astype(F32) * (HEAD_DIM ** (-0.5))
        QZ[half, :HQ, :] = jnp.where(half_lane < HEAD_DIM, qs, 0.0).astype(BF)
        QZ[half, HQ:, :] = jnp.where(half_lane >= HEAD_DIM, qs, 0.0).astype(BF)

    def qcopy():
        return pltpu.make_async_remote_copy(
            src_ref=q_ref.at[pl.ds(HQ, HQ)], dst_ref=QR, send_sem=qsem.at[0], recv_sem=qsem.at[1],
            device_id=(ps, tp), device_id_type=MESH,
        )

    for cp in local[:3]:
        cp.wait()
    pl.semaphore_wait(bar, 19)
    qcopy().start()
    for p in KV:
        begin(p)
    local[4].wait()
    ybegin(oblock, oss, ors)
    spread(0, q_ref[:HQ, :])
    ACC[1] = jnp.zeros((2 * HQ, 256), F32)
    MX[1] = jnp.full((2 * HQ, 128), -1e30, F32)

    def scores(half, s, width, r0=0):
        kb = GK[pl.ds(pl.multiple_of(s * ROWS, ROWS), width), :]
        return lax.dot_general(QZ[half], kb, NT, preferred_element_type=F32)

    def values_of(s, width):
        vb = GV[pl.ds(pl.multiple_of(s * ROWS, ROWS), width), :]
        return jnp.concatenate([vb, jnp.ones((width, 128), BF)], axis=1)

    def attend(half, s, width, first_key, is_first):
        sc = scores(half, s, width)
        tops, wts = [], []
        for h in range(2):
            sh = sc[h * HQ : (h + 1) * HQ] - GG[s, h : h + 1, :width]
            if first_key is not None:
                row = lax.broadcasted_iota(jnp.int32, (HQ, width), 0) + first_key
                col = lax.broadcasted_iota(jnp.int32, (HQ, width), 1)
                sh = jnp.where(col <= row, sh, -1e30)
            top = jnp.max(sh, axis=1, keepdims=True)
            if is_first:
                top = jnp.broadcast_to(top, (HQ, 128))
            else:
                top = jnp.maximum(MX[half, h * HQ : (h + 1) * HQ, :], top)
            wts.append(jnp.exp(sh - jnp.concatenate([top] * (width // 128), axis=1)).astype(BF))
            tops.append(top)
        top = jnp.concatenate(tops, axis=0)
        pv = jnp.dot(jnp.concatenate(wts, axis=0), values_of(s, width), preferred_element_type=F32)
        if is_first:
            ACC[half] = pv
        else:
            fade = jnp.exp(MX[half] - top)
            ACC[half] = ACC[half] * jnp.concatenate([fade, fade], axis=1) + pv
        MX[half] = top

    attend(0, sp, HQ, 0, True)
    qcopy().wait_recv()
    spread(1, QR[...])
    for cp in local[5:7]:
        cp.wait()
    mine = pl.ds(pl.multiple_of(sp * 128, 128), 128)
    for j in range(5):
        GW[mine, j * 256 : j * 256 + 128] = wg_ref[:, j * 128 : (j + 1) * 128]
        GW[mine, j * 256 + 128 : (j + 1) * 256] = wu_ref[:, j * 128 : (j + 1) * 128]
    GW[mine, 1280:1408] = jnp.concatenate(
        [wg_ref[:, 640:], wu_ref[:, 640:], jnp.zeros((128, 32), BF)], axis=1
    )
    local[3].wait()
    for k in range(1, LOOK):
        for p in KV:
            serve(p, k)

    def step(k, _):
        @pl.when((k + LOOK < N_SP) & (k + LOOK > 0))
        def _():
            for p in KV:
                serve(p, k + LOOK)

        @pl.when(k == K_O1)
        def _():
            yserve(oblock, oss, ors, 0)
            yserve(oblock, oss, ors, 1)

        @pl.when(k == K_O2)
        def _():
            yserve(oblock, oss, ors, 2)

        @pl.when(k == K_W)
        def _():
            for p in WEIGHTS:
                begin_first(p)

        @pl.when(k == K_WS)
        def _():
            for p in WEIGHTS:
                serve_first(p, 1)
                serve_first(p, 3)

        s = spof(*offsets(k))

        @pl.when(s < sp)
        def _():
            attend(0, s, ROWS, None, False)

        @pl.when(s < ps)
        def _():
            attend(1, s, ROWS, None, False)

        @pl.when(s == ps)
        def _():
            attend(1, s, ROWS, HQ, False)

        return 0

    lax.fori_loop(0, N_SP, step, 0)

    for half in range(2):
        o0 = ACC[half, :HQ, :128] / ACC[half, :HQ, 128:]
        o1 = ACC[half, HQ:, :128] / ACC[half, HQ:, 128:]
        ATL[half * HQ : (half + 1) * HQ, :] = jnp.where(half_lane < HEAD_DIM, o0, o1).astype(BF)

    def acopy(i, dst, slot):
        return pltpu.make_async_remote_copy(
            src_ref=ATL.at[pl.ds(pl.multiple_of(dst * OWN, 32), OWN)],
            dst_ref=AT.at[:, pl.ds(pl.multiple_of(slot * 128, 128), 128)],
            send_sem=ass.at[i], recv_sem=ars.at[slot],
            device_id=(sp + (dst // 4) * (ps - sp), dst), device_id_type=MESH,
        )

    for i in range(1, 8):
        acopy(i, (tp + i) % 8, tp).start()

    @pl.when(tp >= 4)
    def _():
        acopy(0, tp, tp).start()

    @pl.when(tp < 4)
    def _():
        AT[:, pl.ds(pl.multiple_of(tp * 128, 128), 128)] = ATL[pl.ds(pl.multiple_of(tp * OWN, 32), OWN), :]

    for p in (3, 4):
        serve_first(p, 2)
        for da in (0, 1, 3, 2):
            send_second(p, da)
    yfinish(oblock, oss, ors)
    for cp in local[7:]:
        cp.wait()
    for i in range(1, 8):
        acopy(0, tp, (tp + i) % 8).wait_recv()

    @pl.when(tp >= 4)
    def _():
        acopy(0, tp, tp).wait_recv()

    NB = 512
    sq = jnp.zeros((OWN, 1), F32)
    for j in range(D // NB):
        pj = jnp.dot(AT[...], GO[:, j * NB : (j + 1) * NB], preferred_element_type=F32)
        mj = resid_ref[:, j * NB : (j + 1) * NB].astype(F32) + pj
        MIX[:, j * NB : (j + 1) * NB] = mj
        sq = sq + jnp.sum(mj * mj, axis=1, keepdims=True)
    inv = lax.rsqrt(sq * (1.0 / D) + 1e-6)
    own_slot = slot_of(y, c)
    NA[pl.ds(pl.multiple_of(own_slot * OWN, OWN), OWN), :] = (MIX[...] * inv * gain_ref[...]).astype(BF)
    for h in range(2):
        ybegin(*nblock(h))
    relay(3)
    for p in (5, 6):
        serve_first(p, 2)
        for da in (0, 1, 3, 2):
            send_second(p, da)
    relay(4)
    for n in range(2):
        for h in range(2):
            yserve(*nblock(h), n)
    relay(5)
    for h in range(2):
        yserve(*nblock(h), 2)
    relay(6)
    collect(3)
    collect(4)
    for h in range(2):
        yfinish(*nblock(h))

    def gu(j, _):
        col = pl.multiple_of(j * 256, 256)
        r = jnp.dot(NA[...], GW[:, pl.ds(col, 256)], preferred_element_type=F32)
        gt = r[:, :128]
        HID[:, pl.ds(pl.multiple_of(j * 128, 128), 128)] = (gt / (1.0 + jnp.exp(-gt)) * r[:, 128:]).astype(BF)
        return 0

    lax.fori_loop(0, 5, gu, 0)
    r = jnp.dot(NA[...], GW[:, 1280:1408], preferred_element_type=F32)
    gt = r[:, :48]
    HID[:, 640:688] = (gt / (1.0 + jnp.exp(-gt)) * r[:, 48:96]).astype(BF)
    collect(5)
    collect(6)

    half = 4 * OWN

    def scopy(j):
        view = (slice(None), pl.ds(j * NB, NB))
        return pltpu.make_async_remote_copy(
            src_ref=SB.at[view], dst_ref=RB.at[view], send_sem=bss.at[j], recv_sem=brs.at[j],
            device_id=(sp, sib), device_id_type=MESH,
        )

    def rcopy(n, j, to):
        view = (n, slice(None), pl.ds(j * NB, NB))
        return pltpu.make_async_remote_copy(
            src_ref=TB.at[view], dst_ref=RR.at[view], send_sem=css.at[n, j], recv_sem=crs.at[n, j],
            device_id=(sp, tpof(yat(to), c)), device_id_type=MESH,
        )

    def ocopy(j):
        view = (slice(None), pl.ds(j * NB, NB))
        return pltpu.make_async_copy(out_ref.at[view], out_hbm.at[view], osem.at[j])

    def both(n, j):
        view = (pl.ds(pl.multiple_of(yat(n) * OWN, OWN), OWN), slice(j * NB, (j + 1) * NB))
        return PA[view] + RB[view].astype(F32)

    NC = D // NB
    hs = HID[pl.ds(pl.multiple_of((1 - c) * half, half), half), :]
    ho = HID[pl.ds(pl.multiple_of(c * half, half), half), :]
    for j in range(NC):
        cols = slice(j * NB, (j + 1) * NB)
        SB[:, cols] = jnp.dot(hs, GD[:, cols], preferred_element_type=F32).astype(BF)
        scopy(j).start()
        PA[:, cols] = jnp.dot(ho, GD[:, cols], preferred_element_type=F32)
        if j > 0:
            scopy(j - 1).wait_recv()
            TB[0, :, (j - 1) * NB : j * NB] = both(2, j - 1).astype(BF)
            rcopy(0, j - 1, dy).start()
    scopy(NC - 1).wait_recv()
    TB[0, :, (NC - 1) * NB :] = both(2, NC - 1).astype(BF)
    rcopy(0, NC - 1, dy).start()
    for j in range(NC):
        cols = slice(j * NB, (j + 1) * NB)
        TB[1, :, cols] = both(-dy, j).astype(BF)
        rcopy(1, j, -dy).start()
    for j in range(NC):
        cols = slice(j * NB, (j + 1) * NB)
        rcopy(0, j, dy).wait_recv()
        TB[2, :, cols] = (both(dy, j) + RR[0, :, cols].astype(F32)).astype(BF)
        rcopy(2, j, dy).start()
    for j in range(NC):
        cols = slice(j * NB, (j + 1) * NB)
        rcopy(1, j, -dy).wait_recv()
        rcopy(2, j, dy).wait_recv()
        ffn = both(0, j) + RR[1, :, cols].astype(F32) + RR[2, :, cols].astype(F32)
        out_ref[:, cols] = (MIX[:, cols] + 0.5 * ffn).astype(BF)
        ocopy(j).start()

    for j in range(NC):
        for n in range(3):
            rcopy(n, j, dy).wait_send()
        scopy(j).wait_send()
    for i in range(1, 8):
        acopy(i, tp, tp).wait_send()

    @pl.when(tp >= 4)
    def _():
        acopy(0, tp, tp).wait_send()

    qcopy().wait_send()
    for j in range(NC):
        ocopy(j).wait()
    for i in range(7):
        ycopy(oblock, oss, ors, i, slot_of(y, c), sib).wait_send()
        for h in range(2):
            ycopy(*nblock(h), i, slot_of(y, c), sib).wait_send()
    for p in range(N_PIECE):

        def drain(i, _):
            copy(p, sp, i, sp).wait_send()
            return 0

        lax.fori_loop(0, 15, drain, 0)


def local(resid, queries, keys, values, cum_gate, out_weight, norm_gain, gate_weight, up_weight, down_weight):
    vm = pl.BlockSpec(memory_space=pltpu.VMEM)
    hbm = pl.BlockSpec(memory_space=pl.ANY)
    dma = pltpu.SemaphoreType.DMA
    V = pltpu.VMEM
    return pl.pallas_call(
        kernel,
        out_shape=jax.ShapeDtypeStruct((OWN, D), BF),
        in_specs=[vm] + [hbm] * 9,
        out_specs=hbm,
        scratch_shapes=[
            V((N_SP, 2, ROWS), F32),
            V((N_SP * ROWS, 128), BF),
            V((N_SP * ROWS, 128), BF),
            V((D, GUW), BF),
            V((FFW, D), BF),
            V((1024, D), BF),
            V((HQ, 128), BF),
            V((2, ROWS, 128), BF),
            V((2, ROWS, 256), F32),
            V((2, ROWS, 128), F32),
            V((ROWS, 128), BF),
            V((OWN, 1024), BF),
            V((OWN, D), F32),
            V((ROWS, D), BF),
            V((ROWS, FFW), BF),
            V((4 * OWN, D), BF),
            V((4 * OWN, D), BF),
            V((4 * OWN, D), F32),
            V((3, OWN, D), BF),
            V((3, OWN, D), BF),
            V((128, FFW), BF),
            V((128, FFW), BF),
            V((OWN, D), BF),
            V((1, D), F32),
            V((OWN, D), BF),
            dma((N_PIECE, N_SP)),
            dma((N_PIECE, 15)),
            dma((8,)),
            dma((7,)),
            dma((2, 8)),
            dma((2, 7)),
            dma((8,)),
            dma((8,)),
            dma((4,)),
            dma((4,)),
            dma((3, 4)),
            dma((3, 4)),
            dma((9,)),
            dma((2,)),
            dma((4,)),
        ],
        compiler_params=pltpu.CompilerParams(
            collective_id=0, has_side_effects=True, vmem_limit_bytes=64 * 1024 * 1024 - 128 * 1024
        ),
        name="layer",
    )(
        queries, keys, values, cum_gate.T, out_weight, gate_weight, up_weight, down_weight, resid,
        norm_gain.reshape(1, D),
    )


def solution(mesh):
    return jax.shard_map(
        local,
        mesh=mesh,
        in_specs=(
            P(("sp", "tp"), None),
            P("sp", "tp"),
            P("sp", "tp"),
            P("sp", "tp"),
            P("sp", "tp"),
            P("tp", None),
            P(),
            P("sp", "tp"),
            P("sp", "tp"),
            P("tp", "sp"),
        ),
        out_specs=P(("sp", "tp"), None),
        check_vma=False,
    )
```

time: 150 us -> 127 us (0.85)
  the two profiles are of different devices: /device:TPU:1 before, /device:TPU:32 now
where the time goes in v2:
time: 127 us
  Pallas kernels  123 us (97%)
  local copies, waits for them, and re-layouts  4.37 us (3%)
    pallas_call x1, Pallas kernels, local(): pl.pallas_call(kernel, out_shape=jax.ShapeDtypeStruct((OWN, D), BF), in_s...  123 us
    unnamed x5, local copies, waits for them, and re-layouts  4.37 us

profile of v2, /device:TPU:32, one launch (start us, length us, event | category | flops | bytes accessed | tf_op | source)
XLA Modules:
  0.0 127.1 jit_solution(4081863467405721581)
XLA Ops:
  0.0 0.0 copy-start
  0.0 1.8 %copy.11.wg_in = bf16[128,688]{1,0:T(8,128)(2,1)} copy(bf16[128,688]{0,1:T(8,128)(2,1)} %param.17) | data formatting | bytes 352256 | tf_op args[7]
  1.8 0.0 copy-done
  1.8 0.8 copy.12.wu_in
  2.6 122.7 %layer.1 = bf16[96,2048]{1,0:T(8,128)(2,1)} custom-call(bf16[768,128]{1,0:T(8,128)(2,1)} %q_ref.1, bf16[768,128]{1,0:T(8,128)(2,1)} %k_ref.1, bf16[768,128]{1,0:T(8,128)(2,1)} %v_ref.1, f32[2,768]{1,0:T(2,128)} %bitcast.3, bf16[128,2048]{1,0:T(8,128)(2,1)} %ow_ref.1, bf16[128,688]{1,0:T(8,128)(2,1)} %copy.11.wg_in, bf16[128,688]{1,0:T(8,128)(2,1)} %copy.12.wu_in, ...), custom_call_target="tpu_custom_call" | custom-call | tf_op jit(solution)/shard_map/layer/pallas_call | solution.py:510
  125.3 1.8 %copy.14 = bf16[96,2048]{1,0:T(8,128)(2,1)} copy(bf16[96,2048]{1,0:T(8,128)(2,1)} %layer.1) | data formatting | bytes 786432
Async XLA Ops:
  0.0 1.8 %copy-start = (bf16[128,688]{0,1:T(8,128)(2,1)S(1)}, bf16[128,688]{0,1:T(8,128)(2,1)}, u32[]{:S(2)}) copy-start(bf16[128,688]{0,1:T(8,128)(2,1)} %param.18) | copy-start | bytes 528388

commit v3 on v2

--- a/solution.py
+++ b/solution.py
@@ -12,15 +12,18 @@
 OWN = 96
 D = 2048
 FFW = 688
-GUW = 1408
 N_SP = 16
 HQ = ROWS // 2
+QROWS = 384
+AHEAD = 1
+R5 = 0
+R6 = 2
 KV = (1, 2, 0)
 LOOK = 1
 K_O1 = 6
 K_O2 = 10
-K_W = 5
-K_WS = 12
+K_W = 8
+K_WS = 13
 WEIGHTS = (3, 4, 5, 6)
 BF = jnp.bfloat16
 F32 = jnp.float32
@@ -48,10 +51,10 @@
 
 
 def kernel(
-    q_ref, k_ref, v_ref, g_ref, ow_ref, wg_in, wu_in, wd_ref, resid_in, gain_in,
+    q_in, k_ref, v_ref, g_ref, ow_ref, wg_ref, wu_ref, wd_ref, resid_in, gain_in,
     out_hbm,
-    GG, GK, GV, GW, GD, GO, QR, QZ, ACC, MX, ATL, AT, MIX, NA, HID, SB, RB, PA, TB, RR,
-    wg_ref, wu_ref, resid_ref, gain_ref, out_ref,
+    GG, GK, GV, GT, UT, GD, GO, QR, QZ, ACC, MX, ATL, AT, MIX, NA, HID, SB, RB, PA, TB, RR,
+    q_ref, resid_ref, gain_ref, out_ref,
     rs, ss, ors, oss, nrs, nss, ars, ass, brs, bss, crs, css, lsem, qsem, osem,
 ):
     sp = lax.axis_index("sp")
@@ -88,9 +91,9 @@
         if p == 2:
             return GV.at[pl.ds(pl.multiple_of(s * ROWS, ROWS), ROWS)]
         if p == 3:
-            return GW.at[pl.ds(pl.multiple_of(s * 128, 64), 64)]
+            return GT.at[:, pl.ds(pl.multiple_of(s * 128, 128), 128)]
         if p == 4:
-            return GW.at[pl.ds(pl.multiple_of(s * 128 + 64, 64), 64)]
+            return UT.at[:, pl.ds(pl.multiple_of(s * 128, 128), 128)]
         if p == 5:
             return GD.at[pl.ds(0, 352), pl.ds(pl.multiple_of(s * 128, 128), 128)]
         return GD.at[pl.ds(352, 336), pl.ds(pl.multiple_of(s * 128, 128), 128)]
@@ -101,12 +104,13 @@
         pltpu.make_async_copy(v_ref, part(2, sp), lsem.at[2]),
         pltpu.make_async_copy(wd_ref, GD.at[:, pl.ds(pl.multiple_of(sp * 128, 128), 128)], lsem.at[3]),
         pltpu.make_async_copy(ow_ref, GO.at[pl.ds(pl.multiple_of(tp * 128, 128), 128)], lsem.at[4]),
-        pltpu.make_async_copy(wg_in, wg_ref, lsem.at[5]),
-        pltpu.make_async_copy(wu_in, wu_ref, lsem.at[6]),
+        pltpu.make_async_copy(wg_ref, part(3, sp), lsem.at[5]),
+        pltpu.make_async_copy(wu_ref, part(4, sp), lsem.at[6]),
         pltpu.make_async_copy(resid_in, resid_ref, lsem.at[7]),
         pltpu.make_async_copy(gain_in, gain_ref, lsem.at[8]),
     ]
-    for cp in local:
+    q_local = pltpu.make_async_copy(q_in, q_ref, lsem.at[9])
+    for cp in [q_local] + local:
         cp.start()
 
     def copy(p, s, idx, dst):
@@ -135,17 +139,19 @@
         if da == (4 - d) % 4:
             copy(p, s, 10, spof(d, 0)).start()
 
+    def onward(p, da):
+        return SIGN[p] * (1 - 2 * (da % 2))
+
     def relay(p):
-        d = SIGN[p]
         for da in (0, 1, 3, 2):
+            d = onward(p, da)
             s = spof(da, 4 - d)
             copy(p, s, 0, sp).wait_recv()
             copy(p, s, 11 + da, spof(0, d)).start()
 
     def collect(p):
-        d = SIGN[p]
-        for db in (4 + d, 2):
-            for da in (0, 1, 3, 2):
+        for da in (0, 1, 3, 2):
+            for db in (4 + onward(p, da), 2):
                 copy(p, spof(da, db), 0, sp).wait_recv()
 
     def serve(p, k):
@@ -231,7 +237,7 @@
             device_id=(ps, tp), device_id_type=MESH,
         )
 
-    for cp in local[:3]:
+    for cp in [q_local] + local[:3]:
         cp.wait()
     pl.semaphore_wait(bar, 19)
     qcopy().start()
@@ -243,51 +249,54 @@
     ACC[1] = jnp.zeros((2 * HQ, 256), F32)
     MX[1] = jnp.full((2 * HQ, 128), -1e30, F32)
 
-    def scores(half, s, width, r0=0):
-        kb = GK[pl.ds(pl.multiple_of(s * ROWS, ROWS), width), :]
-        return lax.dot_general(QZ[half], kb, NT, preferred_element_type=F32)
-
     def values_of(s, width):
         vb = GV[pl.ds(pl.multiple_of(s * ROWS, ROWS), width), :]
         return jnp.concatenate([vb, jnp.ones((width, 128), BF)], axis=1)
 
     def attend(half, s, width, first_key, is_first):
-        sc = scores(half, s, width)
-        tops, wts = [], []
-        for h in range(2):
-            sh = sc[h * HQ : (h + 1) * HQ] - GG[s, h : h + 1, :width]
+        kb = GK[pl.ds(pl.multiple_of(s * ROWS, ROWS), width), :]
+        vb = values_of(s, width)
+        count = 2 * HQ // QROWS
+
+        def score(n):
+            return lax.dot_general(
+                QZ[half, n * QROWS : (n + 1) * QROWS, :], kb, NT, preferred_element_type=F32
+            )
+
+        def finish(n, sc):
+            h, r0 = divmod(n * QROWS, HQ)
+            rows = slice(n * QROWS, (n + 1) * QROWS)
+            sh = sc - GG[s, h : h + 1, :width]
             if first_key is not None:
-                row = lax.broadcasted_iota(jnp.int32, (HQ, width), 0) + first_key
-                col = lax.broadcasted_iota(jnp.int32, (HQ, width), 1)
+                row = lax.broadcasted_iota(jnp.int32, (QROWS, width), 0) + (first_key + r0)
+                col = lax.broadcasted_iota(jnp.int32, (QROWS, width), 1)
                 sh = jnp.where(col <= row, sh, -1e30)
             top = jnp.max(sh, axis=1, keepdims=True)
             if is_first:
-                top = jnp.broadcast_to(top, (HQ, 128))
+                top = jnp.broadcast_to(top, (QROWS, 128))
             else:
-                top = jnp.maximum(MX[half, h * HQ : (h + 1) * HQ, :], top)
-            wts.append(jnp.exp(sh - jnp.concatenate([top] * (width // 128), axis=1)).astype(BF))
-            tops.append(top)
-        top = jnp.concatenate(tops, axis=0)
-        pv = jnp.dot(jnp.concatenate(wts, axis=0), values_of(s, width), preferred_element_type=F32)
-        if is_first:
-            ACC[half] = pv
-        else:
-            fade = jnp.exp(MX[half] - top)
-            ACC[half] = ACC[half] * jnp.concatenate([fade, fade], axis=1) + pv
-        MX[half] = top
+                old = MX[half, rows, :]
+                top = jnp.maximum(old, top)
+            wt = jnp.exp(sh - jnp.concatenate([top] * (width // 128), axis=1)).astype(BF)
+            pv = jnp.dot(wt, vb, preferred_element_type=F32)
+            if is_first:
+                ACC[half, rows, :] = pv
+            else:
+                fade = jnp.exp(old - top)
+                ACC[half, rows, :] = ACC[half, rows, :] * jnp.concatenate([fade, fade], axis=1) + pv
+            MX[half, rows, :] = top
+
+        held = [score(n) for n in range(AHEAD)]
+        for n in range(count):
+            if n + AHEAD < count:
+                held.append(score(n + AHEAD))
+            finish(n, held[n])
 
     attend(0, sp, HQ, 0, True)
     qcopy().wait_recv()
     spread(1, QR[...])
     for cp in local[5:7]:
         cp.wait()
-    mine = pl.ds(pl.multiple_of(sp * 128, 128), 128)
-    for j in range(5):
-        GW[mine, j * 256 : j * 256 + 128] = wg_ref[:, j * 128 : (j + 1) * 128]
-        GW[mine, j * 256 + 128 : (j + 1) * 256] = wu_ref[:, j * 128 : (j + 1) * 128]
-    GW[mine, 1280:1408] = jnp.concatenate(
-        [wg_ref[:, 640:], wu_ref[:, 640:], jnp.zeros((128, 32), BF)], axis=1
-    )
     local[3].wait()
     for k in range(1, LOOK):
         for p in KV:
@@ -388,34 +397,43 @@
     for h in range(2):
         ybegin(*nblock(h))
     relay(3)
+    relay(4)
     for p in (5, 6):
         serve_first(p, 2)
         for da in (0, 1, 3, 2):
             send_second(p, da)
-    relay(4)
     for n in range(2):
         for h in range(2):
             yserve(*nblock(h), n)
-    relay(5)
     for h in range(2):
         yserve(*nblock(h), 2)
-    relay(6)
     collect(3)
     collect(4)
     for h in range(2):
         yfinish(*nblock(h))
 
     def gu(j, _):
-        col = pl.multiple_of(j * 256, 256)
-        r = jnp.dot(NA[...], GW[:, pl.ds(col, 256)], preferred_element_type=F32)
-        gt = r[:, :128]
-        HID[:, pl.ds(pl.multiple_of(j * 128, 128), 128)] = (gt / (1.0 + jnp.exp(-gt)) * r[:, 128:]).astype(BF)
+        @pl.when(j == R5)
+        def _():
+            relay(5)
+
+        @pl.when(j == R6)
+        def _():
+            relay(6)
+
+        gate_up(pl.multiple_of(j * 128, 128), 128)
         return 0
 
+    def gate_up(c0, n):
+        rows = pl.ds(c0, n)
+        r = lax.dot_general(
+            NA[...], jnp.concatenate([GT[rows, :], UT[rows, :]], axis=0), NT, preferred_element_type=F32
+        )
+        gt = r[:, :n]
+        HID[:, rows] = (gt / (1.0 + jnp.exp(-gt)) * r[:, n:]).astype(BF)
+
     lax.fori_loop(0, 5, gu, 0)
-    r = jnp.dot(NA[...], GW[:, 1280:1408], preferred_element_type=F32)
-    gt = r[:, :48]
-    HID[:, 640:688] = (gt / (1.0 + jnp.exp(-gt)) * r[:, 48:96]).astype(BF)
+    gate_up(640, 48)
     collect(5)
     collect(6)
 
@@ -462,6 +480,25 @@
         cols = slice(j * NB, (j + 1) * NB)
         TB[1, :, cols] = both(-dy, j).astype(BF)
         rcopy(1, j, -dy).start()
+    for p in range(N_PIECE):
+
+        def drain(i, _):
+            copy(p, sp, i, sp).wait_send()
+            return 0
+
+        lax.fori_loop(0, 15, drain, 0)
+    for i in range(7):
+        ycopy(oblock, oss, ors, i, slot_of(y, c), sib).wait_send()
+        for h in range(2):
+            ycopy(*nblock(h), i, slot_of(y, c), sib).wait_send()
+    for i in range(1, 8):
+        acopy(i, tp, tp).wait_send()
+
+    @pl.when(tp >= 4)
+    def _():
+        acopy(0, tp, tp).wait_send()
+
+    qcopy().wait_send()
     for j in range(NC):
         cols = slice(j * NB, (j + 1) * NB)
         rcopy(0, j, dy).wait_recv()
@@ -479,44 +516,25 @@
         for n in range(3):
             rcopy(n, j, dy).wait_send()
         scopy(j).wait_send()
-    for i in range(1, 8):
-        acopy(i, tp, tp).wait_send()
-
-    @pl.when(tp >= 4)
-    def _():
-        acopy(0, tp, tp).wait_send()
-
-    qcopy().wait_send()
     for j in range(NC):
         ocopy(j).wait()
-    for i in range(7):
-        ycopy(oblock, oss, ors, i, slot_of(y, c), sib).wait_send()
-        for h in range(2):
-            ycopy(*nblock(h), i, slot_of(y, c), sib).wait_send()
-    for p in range(N_PIECE):
-
-        def drain(i, _):
-            copy(p, sp, i, sp).wait_send()
-            return 0
-
-        lax.fori_loop(0, 15, drain, 0)
 
 
 def local(resid, queries, keys, values, cum_gate, out_weight, norm_gain, gate_weight, up_weight, down_weight):
-    vm = pl.BlockSpec(memory_space=pltpu.VMEM)
     hbm = pl.BlockSpec(memory_space=pl.ANY)
     dma = pltpu.SemaphoreType.DMA
     V = pltpu.VMEM
     return pl.pallas_call(
         kernel,
         out_shape=jax.ShapeDtypeStruct((OWN, D), BF),
-        in_specs=[vm] + [hbm] * 9,
+        in_specs=[hbm] * 10,
         out_specs=hbm,
         scratch_shapes=[
             V((N_SP, 2, ROWS), F32),
             V((N_SP * ROWS, 128), BF),
             V((N_SP * ROWS, 128), BF),
-            V((D, GUW), BF),
+            V((FFW, D), BF),
+            V((FFW, D), BF),
             V((FFW, D), BF),
             V((1024, D), BF),
             V((HQ, 128), BF),
@@ -533,8 +551,7 @@
             V((4 * OWN, D), F32),
             V((3, OWN, D), BF),
             V((3, OWN, D), BF),
-            V((128, FFW), BF),
-            V((128, FFW), BF),
+            V((ROWS, 128), BF),
             V((OWN, D), BF),
             V((1, D), F32),
             V((OWN, D), BF),
@@ -550,7 +567,7 @@
             dma((4,)),
             dma((3, 4)),
             dma((3, 4)),
-            dma((9,)),
+            dma((10,)),
             dma((2,)),
             dma((4,)),
         ],
@@ -559,7 +576,7 @@
         ),
         name="layer",
     )(
-        queries, keys, values, cum_gate.T, out_weight, gate_weight, up_weight, down_weight, resid,
+        queries, keys, values, cum_gate.T, out_weight, gate_weight.T, up_weight.T, down_weight, resid,
         norm_gain.reshape(1, D),
     )
 

time: 127 us -> 118 us (0.929)
  the two profiles are of different devices: /device:TPU:32 before, /device:TPU:1 now
where the time goes in v3:
time: 118 us; the launch traced here: 117 us
  Pallas kernels  115 us (97%)
  local copies, waits for them, and re-layouts  1.77 us (2%)
    pallas_call x1, Pallas kernels, local(): pl.pallas_call(kernel, out_shape=jax.ShapeDtypeStruct((OWN, D), BF), in_s...  115 us

profile of v3, /device:TPU:1, one launch (start us, length us, event | category | flops | bytes accessed | tf_op | source)
XLA Modules:
  0.0 116.9 jit_solution(5138072128520314196)
XLA Ops:
  0.0 115.1 %layer.1 = bf16[96,2048]{1,0:T(8,128)(2,1)} custom-call(bf16[768,128]{1,0:T(8,128)(2,1)} %q_in.1, bf16[768,128]{1,0:T(8,128)(2,1)} %k_ref.1, bf16[768,128]{1,0:T(8,128)(2,1)} %v_ref.1, f32[2,768]{1,0:T(2,128)} %bitcast.7, bf16[128,2048]{1,0:T(8,128)(2,1)} %ow_ref.1, bf16[688,128]{1,0:T(8,128)(2,1)} %bitcast.4, bf16[688,128]{1,0:T(8,128)(2,1)} %bitcast.5, ...), custom_call_target="tpu_custom_call" | custom-call | tf_op jit(solution)/shard_map/layer/pallas_call | solution.py:527
  115.1 1.8 %copy.12 = bf16[96,2048]{1,0:T(8,128)(2,1)} copy(bf16[96,2048]{1,0:T(8,128)(2,1)} %layer.1) | data formatting | bytes 786432

commit v4 on v3

--- a/solution.py
+++ b/solution.py
@@ -13,6 +13,8 @@
 D = 2048
 FFW = 688
 N_SP = 16
+NB = 256
+NC = D // NB
 HQ = ROWS // 2
 QROWS = 384
 AHEAD = 1
@@ -20,6 +22,8 @@
 R6 = 2
 KV = (1, 2, 0)
 LOOK = 1
+EARLY = (0,)
+MIXED = False
 K_O1 = 6
 K_O2 = 10
 K_W = 8
@@ -242,7 +246,8 @@
     pl.semaphore_wait(bar, 19)
     qcopy().start()
     for p in KV:
-        begin(p)
+        begin_first(p)
+        send_second(p, 0)
     local[4].wait()
     ybegin(oblock, oss, ors)
     spread(0, q_ref[:HQ, :])
@@ -327,6 +332,9 @@
             for p in WEIGHTS:
                 serve_first(p, 1)
                 serve_first(p, 3)
+                if p < 5:
+                    for da in EARLY:
+                        send_second(p, da)
 
         s = spof(*offsets(k))
 
@@ -372,7 +380,7 @@
 
     for p in (3, 4):
         serve_first(p, 2)
-        for da in (0, 1, 3, 2):
+        for da in (0, 1, 3, 2)[len(EARLY) :]:
             send_second(p, da)
     yfinish(oblock, oss, ors)
     for cp in local[7:]:
@@ -384,7 +392,6 @@
     def _():
         acopy(0, tp, tp).wait_recv()
 
-    NB = 512
     sq = jnp.zeros((OWN, 1), F32)
     for j in range(D // NB):
         pj = jnp.dot(AT[...], GO[:, j * NB : (j + 1) * NB], preferred_element_type=F32)
@@ -397,8 +404,12 @@
     for h in range(2):
         ybegin(*nblock(h))
     relay(3)
+    if MIXED:
+        serve_first(5, 2)
+        for da in (0, 1, 3, 2):
+            send_second(5, da)
     relay(4)
-    for p in (5, 6):
+    for p in (6,) if MIXED else (5, 6):
         serve_first(p, 2)
         for da in (0, 1, 3, 2):
             send_second(p, da)
@@ -461,25 +472,24 @@
         view = (pl.ds(pl.multiple_of(yat(n) * OWN, OWN), OWN), slice(j * NB, (j + 1) * NB))
         return PA[view] + RB[view].astype(F32)
 
-    NC = D // NB
     hs = HID[pl.ds(pl.multiple_of((1 - c) * half, half), half), :]
     ho = HID[pl.ds(pl.multiple_of(c * half, half), half), :]
+    def pass_on(j):
+        cols = slice(j * NB, (j + 1) * NB)
+        scopy(j).wait_recv()
+        TB[0, :, cols] = both(2, j).astype(BF)
+        rcopy(0, j, dy).start()
+        TB[1, :, cols] = both(-dy, j).astype(BF)
+        rcopy(1, j, -dy).start()
+
     for j in range(NC):
         cols = slice(j * NB, (j + 1) * NB)
         SB[:, cols] = jnp.dot(hs, GD[:, cols], preferred_element_type=F32).astype(BF)
         scopy(j).start()
         PA[:, cols] = jnp.dot(ho, GD[:, cols], preferred_element_type=F32)
         if j > 0:
-            scopy(j - 1).wait_recv()
-            TB[0, :, (j - 1) * NB : j * NB] = both(2, j - 1).astype(BF)
-            rcopy(0, j - 1, dy).start()
-    scopy(NC - 1).wait_recv()
-    TB[0, :, (NC - 1) * NB :] = both(2, NC - 1).astype(BF)
-    rcopy(0, NC - 1, dy).start()
-    for j in range(NC):
-        cols = slice(j * NB, (j + 1) * NB)
-        TB[1, :, cols] = both(-dy, j).astype(BF)
-        rcopy(1, j, -dy).start()
+            pass_on(j - 1)
+    pass_on(NC - 1)
     for p in range(N_PIECE):
 
         def drain(i, _):
@@ -563,13 +573,13 @@
             dma((2, 7)),
             dma((8,)),
             dma((8,)),
-            dma((4,)),
-            dma((4,)),
-            dma((3, 4)),
-            dma((3, 4)),
+            dma((NC,)),
+            dma((NC,)),
+            dma((3, NC)),
+            dma((3, NC)),
             dma((10,)),
             dma((2,)),
-            dma((4,)),
+            dma((NC,)),
         ],
         compiler_params=pltpu.CompilerParams(
             collective_id=0, has_side_effects=True, vmem_limit_bytes=64 * 1024 * 1024 - 128 * 1024

time: 118 us -> 113 us (0.958)
  Pallas kernels: 115 us -> 111 us
    pallas_call x1, Pallas kernels: 115 us -> 111 us  [local(): pl.pallas_call(kernel, out_shape=jax.ShapeDtypeStruct((OWN, D), BF), in_s...]
where the time goes in v4:
time: 113 us; the launch traced here: 112 us
  Pallas kernels  111 us (98%)
  local copies, waits for them, and re-layouts  1.77 us (2%)
    pallas_call x1, Pallas kernels, local(): pl.pallas_call(kernel, out_shape=jax.ShapeDtypeStruct((OWN, D), BF), in_s...  111 us

profile of v4, /device:TPU:1, one launch (start us, length us, event | category | flops | bytes accessed | tf_op | source)
XLA Modules:
  0.0 112.5 jit_solution(16757086817502502875)
XLA Ops:
  0.0 110.7 %layer.1 = bf16[96,2048]{1,0:T(8,128)(2,1)} custom-call(bf16[768,128]{1,0:T(8,128)(2,1)} %q_in.1, bf16[768,128]{1,0:T(8,128)(2,1)} %k_ref.1, bf16[768,128]{1,0:T(8,128)(2,1)} %v_ref.1, f32[2,768]{1,0:T(2,128)} %bitcast.7, bf16[128,2048]{1,0:T(8,128)(2,1)} %ow_ref.1, bf16[688,128]{1,0:T(8,128)(2,1)} %bitcast.4, bf16[688,128]{1,0:T(8,128)(2,1)} %bitcast.5, ...), custom_call_target="tpu_custom_call" | custom-call | tf_op jit(solution)/shard_map/layer/pallas_call | solution.py:537
  110.7 1.8 %copy.12 = bf16[96,2048]{1,0:T(8,128)(2,1)} copy(bf16[96,2048]{1,0:T(8,128)(2,1)} %layer.1) | data formatting | bytes 786432

commit v5 on v4

--- a/solution.py
+++ b/solution.py
@@ -21,7 +21,7 @@
 R5 = 0
 R6 = 2
 KV = (1, 2, 0)
-LOOK = 1
+LOOK = 0
 EARLY = (0,)
 MIXED = False
 K_O1 = 6
@@ -515,6 +515,10 @@
         TB[2, :, cols] = (both(dy, j) + RR[0, :, cols].astype(F32)).astype(BF)
         rcopy(2, j, dy).start()
     for j in range(NC):
+        scopy(j).wait_send()
+        for n in range(2):
+            rcopy(n, j, dy).wait_send()
+    for j in range(NC):
         cols = slice(j * NB, (j + 1) * NB)
         rcopy(1, j, -dy).wait_recv()
         rcopy(2, j, dy).wait_recv()
@@ -523,9 +527,7 @@
         ocopy(j).start()
 
     for j in range(NC):
-        for n in range(3):
-            rcopy(n, j, dy).wait_send()
-        scopy(j).wait_send()
+        rcopy(2, j, dy).wait_send()
     for j in range(NC):
         ocopy(j).wait()
 

time: 113 us -> 113 us (level)
  no operation moved by 1% of the time
where the time goes in v5:
time: 113 us
  Pallas kernels  111 us (98%)
  local copies, waits for them, and re-layouts  1.77 us (2%)
    pallas_call x1, Pallas kernels, local(): pl.pallas_call(kernel, out_shape=jax.ShapeDtypeStruct((OWN, D), BF), in_s...  111 us

profile of v5, /device:TPU:1, one launch (start us, length us, event | category | flops | bytes accessed | tf_op | source)
XLA Modules:
  0.0 112.7 jit_solution(16279902559795923452)
XLA Ops:
  0.0 110.9 %layer.1 = bf16[96,2048]{1,0:T(8,128)(2,1)} custom-call(bf16[768,128]{1,0:T(8,128)(2,1)} %q_in.1, bf16[768,128]{1,0:T(8,128)(2,1)} %k_ref.1, bf16[768,128]{1,0:T(8,128)(2,1)} %v_ref.1, f32[2,768]{1,0:T(2,128)} %bitcast.7, bf16[128,2048]{1,0:T(8,128)(2,1)} %ow_ref.1, bf16[688,128]{1,0:T(8,128)(2,1)} %bitcast.4, bf16[688,128]{1,0:T(8,128)(2,1)} %bitcast.5, ...), custom_call_target="tpu_custom_call" | custom-call | tf_op jit(solution)/shard_map/layer/pallas_call | solution.py:539
  110.9 1.8 %copy.12 = bf16[96,2048]{1,0:T(8,128)(2,1)} copy(bf16[96,2048]{1,0:T(8,128)(2,1)} %layer.1) | data formatting | bytes 786432
